TPU v7x, 128 devices: a whole 4x4x4 slice. The times are simulated.
128 devices in a mesh: sp: 64 (over z, y, x), tp: 2 (over core).
Axes of the slice: x: 4, y: 4, z: 4, core: 2. Of those that a mesh axis runs over, the one named last changes fastest.
Arguments:
- residual: bfloat16 [16384, 2048], P(('sp', 'tp')), may hold values from -6 to 6
- queries: bfloat16 [16384, 1152], P('sp', 'tp'), may hold values from -800 to 800
- latent: bfloat16 [16384, 256], P('sp'), may hold values from -6 to 6
- rope_key: bfloat16 [16384, 32], P('sp'), may hold values from -6 to 6
- doc_ids: int32 [16384], P('sp'), may hold values from 0 to 5, never falling along the last dimension, each value on 1 to 8192 neighbouring positions
- latent_to_key: bfloat16 [256, 768], P(None, 'tp'), may hold values from -0.375 to 0.375
- latent_to_value: bfloat16 [256, 768], P(None, 'tp'), may hold values from -0.375 to 0.375
- out_proj: bfloat16 [768, 2048], replicated, may hold values from -0.21875 to 0.21875
- mix_gain: float32 [2048], replicated, may hold values from 0.1 to 1.9
- moe_gain: float32 [2048], replicated, may hold values from 0.1 to 1.9
- expert_ids: int32 [16384, 2], P(('sp', 'tp')), may hold values from 0 to 63, as said below
- route_weight: float32 [16384, 2], P(('sp', 'tp')), may hold values from 0.1 to 1
- gate_weight: bfloat16 [64, 2048, 1024], P('sp', None, 'tp'), may hold values from -0.125 to 0.125
- up_weight: bfloat16 [64, 2048, 1024], P('sp', None, 'tp'), may hold values from -0.125 to 0.125
- down_weight: bfloat16 [64, 1024, 2048], P('sp', 'tp'), may hold values from -0.1875 to 0.1875
Outputs:
- output: bfloat16 [16384, 2048], P(('sp', 'tp'))
Inputs may be any that keep to these rules, and one draw needn't show every extreme that they name: `expert_ids`: each row names 2 different experts of one group of 16 consecutive numbers; in each aligned block of 128 rows (the rows of one device) no expert is named more than 8 times, and some expert exactly 8 times.
All inputs are finite; a program needn't handle non-finite values.
Results may differ from a plain program's by a relative error of at most 0.013.
Values may be sent and summed in bfloat16 or wider, within the bound.
A program may use at most 64 MiB of HBM per device.

v0:
```python
import math

import jax
import jax.numpy as jnp
from jax import lax
from jax.sharding import PartitionSpec as P

D = 2048
UNROTATED_DIM = 64
ROPE = 32
VALUE_ENTRIES = 64
GROUPS = 4


rope_base = 10000.0
epsilon = 1e-06


def in_order(pieces, dim):
    pieces = jnp.moveaxis(pieces, 0, dim)
    lengths = pieces.shape
    return pieces.reshape(*lengths[:dim], lengths[dim] * lengths[dim + 1], *lengths[dim + 2 :])


def sent_to_all(x, axis):
    size = lax.axis_size(axis)
    return lax.all_to_all(jnp.broadcast_to(x[None], (size, *x.shape)), axis, 0, 0, tiled=True)


def collect(x, axis, dim):
    return in_order(sent_to_all(x, axis), dim)


def cut_along(x, dim, size):
    before, after = (x.shape[:dim], x.shape[dim + 1 :])
    return jnp.moveaxis(x.reshape(*before, size, -1, *after), dim, 0)


def sum_at_owner(x, axis, dim):
    pieces = cut_along(x, dim, lax.axis_size(axis))
    arrived = lax.all_to_all(pieces, axis, split_axis=0, concat_axis=0, tiled=True)
    return arrived.astype(jnp.float32).sum(axis=0)


def rotate(source, positions):
    half_width = source.shape[-1] // 2
    frequency = rope_base ** (-jnp.arange(half_width, dtype=jnp.float32) / half_width)
    angles = positions.astype(jnp.float32)[:, None] * frequency[None, :]
    if source.ndim == 3:
        angles = angles[:, None, :]
    cosine = jnp.cos(angles)
    sine_part = jnp.sin(angles)
    upper_half = source[..., :half_width].astype(jnp.float32)
    lower_half = source[..., half_width:].astype(jnp.float32)
    turned = jnp.concatenate(
        [
            upper_half * cosine - lower_half * sine_part,
            lower_half * cosine + upper_half * sine_part,
        ],
        axis=-1,
    )
    return turned.astype(jnp.bfloat16)


def rms_scale(source, gain):
    return source * lax.rsqrt(jnp.mean(source * source, axis=-1, keepdims=True) + epsilon) * gain


def attend_keys(
    running,
    query_nope,
    query_rot,
    query_pos,
    query_docs,
    key_nope,
    key_rot,
    value_rows,
    key_pos,
    key_docs,
):
    row_max, row_total, weighted = running
    score_scale = (UNROTATED_DIM + ROPE) ** (-0.5)
    scores = (
        jnp.einsum("qhd,khd->qhk", query_nope, key_nope, preferred_element_type=jnp.float32)
        + jnp.einsum("qhr,kr->qhk", query_rot, key_rot, preferred_element_type=jnp.float32)
    ) * score_scale
    allowed = (
        (key_pos[None, :] <= query_pos[:, None]) & (key_docs[None, :] == query_docs[:, None])
    )[:, None, :]
    new_max = jnp.maximum(row_max, jnp.max(jnp.where(allowed, scores, -1e30), axis=-1))
    weights = jnp.where(allowed, jnp.exp(scores - new_max[..., None]), 0.0)
    factor = jnp.exp(row_max - new_max)
    row_total = row_total * factor + jnp.sum(weights, axis=-1)
    weighted = weighted * factor[..., None] + jnp.einsum(
        "qhk,khd->qhd", weights.astype(jnp.bfloat16), value_rows, preferred_element_type=jnp.float32
    )
    return (new_max, row_total, weighted)


def local(
    residual,
    queries,
    latent,
    rope_key,
    doc_ids,
    latent_to_key,
    latent_to_value,
    out_proj,
    mix_gain,
    moe_gain,
    expert_ids,
    route_weight,
    gate_weight,
    up_weight,
    down_weight,
):
    local_rows = queries.shape[0]
    local_heads = queries.shape[1] // (UNROTATED_DIM + ROPE)
    query_pos = lax.axis_index("sp") * local_rows + jnp.arange(local_rows, dtype=jnp.int32)
    shaped = queries.reshape(local_rows, local_heads, UNROTATED_DIM + ROPE)
    query_nope = shaped[..., :UNROTATED_DIM]
    query_rot = rotate(shaped[..., UNROTATED_DIM:], query_pos)
    key_rot = rotate(rope_key, query_pos)
    initial = (
        jnp.full((local_rows, local_heads), -1e30, jnp.float32),
        jnp.zeros((local_rows, local_heads), jnp.float32),
        jnp.zeros((local_rows, local_heads, VALUE_ENTRIES), jnp.float32),
    )
    pieces = (
        lax.all_gather(latent, "sp", axis=0, tiled=True),
        lax.all_gather(key_rot, "sp", axis=0, tiled=True),
        lax.all_gather(doc_ids, "sp", axis=0, tiled=True),
    )
    row_count = pieces[0].shape[0]
    block_rows = math.gcd(row_count, 512)

    def one_block(number, current):
        first_row = number * block_rows
        sliced = [lax.dynamic_slice_in_dim(member, first_row, block_rows, 0) for member in pieces]
        key_pos = first_row + jnp.arange(block_rows, dtype=jnp.int32)
        active = (first_row <= query_pos[-1]) & (sliced[-1][-1] >= doc_ids[0])

        def compute(carried):
            key_nope = jnp.dot(sliced[0], latent_to_key, preferred_element_type=jnp.float32).astype(
                jnp.bfloat16
            )
            value_rows = jnp.dot(
                sliced[0], latent_to_value, preferred_element_type=jnp.float32
            ).astype(jnp.bfloat16)
            key_part = sliced[1]
            return attend_keys(
                carried,
                query_nope,
                query_rot,
                query_pos,
                doc_ids,
                key_nope.reshape(block_rows, local_heads, UNROTATED_DIM),
                key_part,
                value_rows.reshape(block_rows, local_heads, VALUE_ENTRIES),
                key_pos,
                sliced[-1],
            )

        return lax.cond(active, compute, lambda carried: carried, current)

    running = lax.fori_loop(0, row_count // block_rows, one_block, initial)
    attended = (running[2] / running[1][..., None]).astype(jnp.bfloat16)
    attended = attended.reshape(local_rows, local_heads * VALUE_ENTRIES)
    gathered = lax.all_to_all(attended, "tp", split_axis=0, concat_axis=1, tiled=True)
    mix = jnp.dot(gathered, out_proj, preferred_element_type=jnp.float32)
    branch = rms_scale(mix, mix_gain)
    middle = lax.optimization_barrier((residual.astype(jnp.float32) + branch).astype(jnp.bfloat16))
    normed = rms_scale(middle.astype(jnp.float32), moe_gain).astype(jnp.bfloat16)
    row_count = normed.shape[0]
    top_count = expert_ids.shape[1]
    expert_count = lax.axis_size("sp")
    capacity = row_count // (expert_count // GROUPS)
    flat_ids = expert_ids.reshape(-1)
    onehot = (flat_ids[:, None] == jnp.arange(expert_count, dtype=jnp.int32)[None, :]).astype(
        jnp.int32
    )
    earlier = jnp.cumsum(onehot, axis=0) - onehot
    slot_rank = jnp.sum(earlier * onehot, axis=1)
    slot_ids = (flat_ids * capacity + slot_rank).reshape(row_count, top_count)
    chooser = jnp.any(
        jnp.arange(expert_count * capacity, dtype=jnp.int32)[:, None, None] == slot_ids[None],
        axis=2,
    ).astype(jnp.bfloat16)
    buffer = jnp.dot(chooser, normed, preferred_element_type=jnp.float32).astype(jnp.bfloat16)
    buffer = buffer.reshape(expert_count, capacity, D)
    arrived = lax.all_to_all(buffer, "sp", split_axis=0, concat_axis=0, tiled=True)
    model_width = arrived.shape[2]
    both_halves = collect(arrived, "tp", 0)
    flat_rows = both_halves.reshape(-1, model_width)
    gate_out = jnp.dot(flat_rows, gate_weight[0], preferred_element_type=jnp.float32)
    upward = jnp.dot(flat_rows, up_weight[0], preferred_element_type=jnp.float32)
    hidden = (jax.nn.silu(gate_out) * upward).astype(jnp.bfloat16)
    partial_value = jnp.dot(hidden, down_weight[0], preferred_element_type=jnp.float32).reshape(
        both_halves.shape
    )
    summed = sum_at_owner(partial_value.astype(jnp.bfloat16), "tp", 0).astype(jnp.bfloat16)
    returned = lax.all_to_all(summed, "sp", split_axis=0, concat_axis=0, tiled=True)
    picked = returned.reshape(-1, D)[slot_ids.reshape(-1)].astype(jnp.float32)
    expert_mix = jnp.sum(
        (picked * route_weight.reshape(-1)[:, None]).reshape(row_count, top_count, D), axis=1
    )
    return (middle.astype(jnp.float32) + expert_mix).astype(jnp.bfloat16)


def solution(mesh):
    in_specs = (
        P(("sp", "tp"), None),
        P("sp", "tp"),
        P("sp", None),
        P("sp", None),
        P("sp"),
        P(None, "tp"),
        P(None, "tp"),
        P(),
        P(),
        P(),
        P(("sp", "tp"), None),
        P(("sp", "tp"), None),
        P("sp", None, "tp"),
        P("sp", None, "tp"),
        P("sp", "tp", None),
    )
    out_specs = P(("sp", "tp"), None)
    return jax.shard_map(local, mesh=mesh, in_specs=in_specs, out_specs=out_specs, check_vma=False)
```

profile of v0, /device:TPU:1, one launch (start us, length us, event | category | flops | bytes accessed | tf_op | source)
XLA Modules:
  0.0 637.0 jit_solution(9027320513454528965)
XLA Ops:
  10.0 1.6 slice.54
  13.5 159.0 %all-gather = s32[64,1,256]{2,1,0:T(1,128)} all-gather(s32[1,1,256]{2,1,0:T(1,128)} %bitcast.92), channel_id=1, replica_groups=mesh['sp'=64,'tp'=2] {'sp'}, dimensions={0}, use_global_device_ids=true | all-gather | bytes 66560 | tf_op jit(solution)/shard_map/all_gather | solution.py:132
  175.3 216.7 %while.17 = (s32[]{:T(128)}, f32[256,6]{0,1:T(8,128)S(1)}, f32[256,6]{0,1:T(8,128)S(1)}, f32[256,6,64]{0,2,1:T(8,128)S(1)}, s32[256]{0:T(256)}, /*index=5*/s32[1...) while((s32[]{:T(128)}, f32[256,6]{0,1:T(8,128)S(1)}, ...), condition=%wide.region_5.6_spmd, body=%wide.region_0.5_spmd.sunk | while | flops 461835776 | bytes 21579896 | solution.py:166
  179.8 1.3 slice.70
  181.8 7.0 %conditional.2 = ((f32[256,6]{0,1:T(8,128)S(1)}, f32[256,6]{0,1:T(8,128)S(1)}, f32[256,6,64]{0,2,1:T(8,128)S(1)})) conditional(s32[]{:T(128)} %convert_element_type.177, (f32[256,6]{0,1:T(8,128)S(1)}, f32[256,6]{0,1:T(8,128)S(1)}, f32[256,6,64]{0,2,1:T(8,128)S(1)}) %tuple.50, (s32[]{:T(128)}, s32[512]{0:T(512)}, s32[256]{0:T(256)}, s32[512]{0:T(512)}, ...), branch_computations={%region_1.0_spmd, %region_2.4_spmd} | conditional | flops 461835776 | bytes 21565132 | solution.py:164
  181.9 1.4 convolution_convert_fusion.1
  183.2 1.5 fusion.16
  193.3 1.3 slice.70
  199.9 1.3 slice.70
  206.4 1.3 slice.70
  393.8 32.7 %all_to_all.39 = bf16[2,128,384]{1,2,0:T(8,128)(2,1)S(1)} all-to-all(bf16[2,128,384]{1,2,0:T(8,128)(2,1)S(1)} %copy.58), channel_id=1, replica_groups=mesh['sp'=64,'tp'=2] {'tp'}, dimensions={0} | all-to-all | bytes 393216 | tf_op jit(solution)/shard_map/all_to_all | solution.py:169
  429.0 123.3 %all_to_all.40 = bf16[64,8,2048]{2,1,0:T(8,128)(2,1)S(1)} all-to-all(bf16[64,8,2048]{2,1,0:T(8,128)(2,1)S(1)} %fusion.23), channel_id=1, replica_groups=mesh['sp'=64,'tp'=2] {'sp'}, dimensions={0} | all-to-all | bytes 4194304 | tf_op jit(solution)/shard_map/all_to_all | solution.py:191
  552.9 9.0 %all_to_all.41 = bf16[2,64,8,2048]{3,2,1,0:T(8,128)(2,1)S(1)} all-to-all(bf16[2,64,8,2048]{3,2,1,0:T(8,128)(2,1)S(1)} %broadcast_in_dim.63), channel_id=1, replica_groups=mesh['sp'=64,'tp'=2] {'tp'}, dimensions={0} | all-to-all | bytes 8388608 | tf_op jit(solution)/shard_map/all_to_all | solution.py:27
  561.9 2.3 fusion.25
  564.2 2.6 fusion.31
  566.9 2.4 convolution_convert_fusion.2
  569.8 8.1 %all_to_all.42 = bf16[2,64,8,2048]{3,1,2,0:T(8,128)(2,1)} all-to-all(bf16[2,64,8,2048]{3,1,2,0:T(8,128)(2,1)S(1)} %copy.65), channel_id=1, replica_groups=mesh['sp'=64,'tp'=2] {'tp'}, dimensions={0} | all-to-all | bytes 8388608 | tf_op jit(solution)/shard_map/all_to_all | solution.py:41
  577.9 3.5 reduce_sum.67
  581.4 2.5 copy.67
  583.9 5.8 all-to-all-start.4
  590.0 28.5 %all-to-all-done.4 = bf16[64,8,2048]{2,1,0:T(8,128)(2,1)S(1)} async-done(((bf16[64,8,2048]{2,1,0:T(8,128)(2,1)}), bf16[64,8,2048]{2,1,0:T(8,128)(2,1)S(1)}, u32[]{:S(2)}, u32[]{:S(2)}) %all-to-all-start.4) | async-done | bytes 2097184 | tf_op jit(solution)/shard_map/all_to_all | solution.py:202
  618.5 2.3 gather_fusion
  620.8 3.5 reshape.226
  624.4 4.9 multiply_reduce_fusion
  (347 shorter events, 159.0 us)
Async XLA Ops:
  6.5 419.9 %copy-start = (bf16[768,2048]{1,0:T(8,128)(2,1)S(1)}, bf16[768,2048]{1,0:T(8,128)(2,1)}, u32[]{:S(2)}) copy-start(bf16[768,2048]{1,0:T(8,128)(2,1)} %param.26) | copy-start | bytes 9437188
  6.5 168.7 %all-gather.6.cloned.1.call-start = ((), (), s32[]{:S(2)}) async-start(), calls=%async_computation.6 | async-start | bytes 1064960 | tf_op jit(solution)/shard_map/all_gather | solution.py:131
  8.2 167.0 %all-gather.4.cloned.1.call-start = ((), (), s32[]{:S(2)}) async-start(), calls=%async_computation.5 | async-start | bytes 8519680 | tf_op jit(solution)/shard_map/all_gather | solution.py:130
  12.6 162.6 %copy-start.14 = (s32[256]{0:T(256)}, s32[256]{0:T(256)S(1)}, u32[]{:S(2)}) copy-start(s32[256]{0:T(256)S(1)} %fusion.49) | copy-start | bytes 3076
  181.8 2.9 copy-start.11
  181.8 2.9 copy-start.10
  181.9 2.9 copy-start.12
  181.9 2.9 copy-start.13
  181.9 3.1 copy-start.4
  185.9 0.9 copy-start.5
  392.0 35.1 %copy-start.16 = (f32[2048]{0:T(1024)S(1)}, f32[2048]{0:T(1024)}, u32[]{:S(2)}) copy-start(f32[2048]{0:T(1024)} %param.27) | copy-start | bytes 24580
  393.7 33.4 %copy-start.6 = (bf16[128,2048]{1,0:T(8,128)(2,1)S(1)}, bf16[128,2048]{1,0:T(8,128)(2,1)}, u32[]{:S(2)}) copy-start(bf16[128,2048]{1,0:T(8,128)(2,1)} %param.19) | copy-start | bytes 1572868
  426.5 1.7 copy-start.7
  426.5 1.7 copy-start.17
  427.4 0.8 copy-start.2
  552.9 9.0 %copy-start.19 = (bf16[1,2048,512]{2,1,0:T(8,128)(2,1)S(1)}, bf16[1,2048,512]{2,1,0:T(8,128)(2,1)}, u32[]{:S(2)}) copy-start(bf16[1,2048,512]{2,1,0:T(8,128)(2,1)} %param.32) | copy-start | bytes 6291460
  561.9 2.3 copy-start.20
  564.2 2.7 copy-start.21
  583.9 5.8 copy-start.8
  583.9 5.9 copy-start.18
  583.9 6.1 copy-start.15
  583.9 34.5 %all-to-all-start.4 = ((bf16[64,8,2048]{2,1,0:T(8,128)(2,1)}), bf16[64,8,2048]{2,1,0:T(8,128)(2,1)S(1)}, u32[]{:S(2)}, u32[]{:S(2)}) async-start(bf16[64,8,2048]{2,1,0:T(8,128)(2,1)} %copy.67), calls=%async_computation.4 | async-start | bytes 4194304 | tf_op jit(solution)/shard_map/all_to_all | solution.py:202
  620.8 9.3 %copy-start.1 = (bf16[768,2048]{1,0:T(8,128)(2,1)S(1)}, bf16[768,2048]{1,0:T(8,128)(2,1)}, u32[]{:S(2)}) copy-start(bf16[768,2048]{1,0:T(8,128)(2,1)} %param.26) | copy-start | bytes 9437188
  624.4 4.9 copy-start.3
  (32 other events, 19.2 us)
Sparse Core Ops, SparseCore 0:
  10.0 65.2 all-gather.5
  78.2 77.8 all-gather.3
where the time goes:
time: 649 us; the launch traced here: 637 us
  blocking collectives  332 us (51%)
  local copies, waits for them, and re-layouts  160 us (25%)
  loops' own time  64.4 us (10%)
  waiting for transfers between devices  29.2 us (4%)
  other arithmetic  17 us (3%)
  matrix products  14.5 us (2%)
  between operations  13.7 us (2%)
    all_gather x1, blocking collectives, local(): lax.all_gather(doc_ids, 'sp', axis=0, tiled=True)  159 us
    all_to_all x1, blocking collectives, local(): lax.all_to_all(buffer, 'sp', split_axis=0, concat_axis=0, tiled=True)  123 us
    slice x96, local copies, waits for them, and re-layouts, one_block(): active = (first_row <= query_pos[-1]) & (sliced[-1][-1] >= doc_ids[0])  102 us
    another operation x1, loops' own time, local(): running = lax.fori_loop(0, row_count // block_rows, one_block, initial)  63.9 us
    all_to_all x1, blocking collectives, local(): lax.all_to_all(attended, 'tp', split_axis=0, concat_axis=1, tiled=True)  32.7 us
    all_to_all x1, waiting for transfers between devices, local(): lax.all_to_all(summed, 'sp', split_axis=0, concat_axis=0, tiled=True)  28.5 us
    dynamic_slice x32, local copies, waits for them, and re-layouts, one_block(): lax.dynamic_slice_in_dim(member, first_row, block_rows, 0)  24.2 us
    iota x32, local copies, waits for them, and re-layouts, one_block(): key_pos = first_row + jnp.arange(block_rows, dtype=jnp.int32)  19.1 us
  transfers between devices with their start and end apart: 3, of which 1 were waited for; matrix products, arithmetic and copies ran while one was open for 1% of the time, Pallas kernels for 0%

commit v1 on v0

v1 whole, which is shorter than its diff:
```python
import functools

import jax
import jax.numpy as jnp
from jax import lax
from jax.experimental import pallas as pl
from jax.experimental.pallas import tpu as pltpu
from jax.sharding import PartitionSpec as P

D = 2048
UNROTATED_DIM = 64
ROPE = 32
HEADS = 6
LATENT = 256
ROWS = 256
HALF = 128
PIECE = 160
EXPERTS = 64
CAP = 8
FF_HALF = 512
PLANE = 16
DEPTH = 4
rope_base = 10000.0
epsilon = 1e-06
MASKED = 1e30
SCORE_BASE2 = float((UNROTATED_DIM + ROPE) ** (-0.5) * 1.4426950408889634)
MESH = pl.DeviceIdType.MESH


def rotate(source, cosine, sine_part):
    half_width = source.shape[-1] // 2
    upper_half = source[..., :half_width].astype(jnp.float32)
    lower_half = source[..., half_width:].astype(jnp.float32)
    turned = jnp.concatenate(
        [
            upper_half * cosine - lower_half * sine_part,
            lower_half * cosine + upper_half * sine_part,
        ],
        axis=-1,
    )
    return turned.astype(jnp.bfloat16)


def nn(a, b):
    return lax.dot_general(a, b, (((1,), (0,)), ((), ())), preferred_element_type=jnp.float32)


def nt(a, b):
    return lax.dot_general(a, b, (((1,), (1,)), ((), ())), preferred_element_type=jnp.float32)


def kernel(
    query_ref,
    own_ref,
    key_w_ref,
    value_w_ref,
    residual_ref,
    mix_gain_ref,
    moe_gain_ref,
    ids_ref,
    ids_t_ref,
    route_ref,
    proj_hbm,
    gate_hbm,
    up_hbm,
    down_hbm,
    out_ref,
    kv,
    run_max,
    run_sum,
    run_out,
    turned_out,
    heads_buf,
    proj,
    gate_w,
    up_w,
    down_w,
    mix,
    middle,
    normed,
    send_buf,
    recv_buf,
    done_buf,
    back_buf,
    z_send,
    plane_send,
    pass_send,
    got,
    passed,
    weight_local,
    weight_send,
    weight_got,
    heads_send,
    heads_got,
    go_send,
    go_got,
    own_copy,
    back_send,
    back_got,
):
    sp = lax.axis_index("sp")
    tp = lax.axis_index("tp")
    other = 1 - tp
    z = sp // PLANE
    me = sp % PLANE

    def remote(src, dst, send_sem, recv_sem, device):
        return pltpu.make_async_remote_copy(
            src_ref=src,
            dst_ref=dst,
            send_sem=send_sem,
            recv_sem=recv_sem,
            device_id=device,
            device_id_type=MESH,
        )

    barrier = pltpu.get_barrier_semaphore()
    pl.semaphore_signal(barrier, inc=1, device_id=(sp, other), device_id_type=MESH)

    def greet(step, carry):
        pl.semaphore_signal(
            barrier, inc=1, device_id=((sp + step) % EXPERTS, tp), device_id_type=MESH
        )
        return carry

    lax.fori_loop(1, EXPERTS, greet, 0)

    local_copies = [
        pltpu.make_async_copy(proj_hbm, proj, weight_local.at[0]),
        pltpu.make_async_copy(gate_hbm.at[0], gate_w.at[tp], weight_local.at[1]),
        pltpu.make_async_copy(up_hbm.at[0], up_w.at[tp], weight_local.at[2]),
        pltpu.make_async_copy(down_hbm.at[0], down_w.at[tp], weight_local.at[3]),
    ]
    for copy in local_copies:
        copy.start()

    pl.semaphore_wait(barrier, EXPERTS)

    next_z = []
    for hop in (1, 2):
        target = ((z + hop) % DEPTH) * PLANE + me
        copy = remote(
            own_ref.at[tp],
            kv.at[hop - 1, me, tp],
            z_send.at[hop - 1],
            got.at[hop - 1, me],
            (target, tp),
        )
        copy.start()
        next_z.append(copy)

    def plane_copy(kind, step, own):
        peer = (me + step) % PLANE
        return remote(
            own_ref.at[tp] if own else kv.at[kind, me, tp],
            kv.at[kind, me, tp],
            plane_send.at[kind, step],
            got.at[kind, me],
            (z * PLANE + peer, tp),
        )

    def send_own(step, carry):
        @pl.when((me + step) % PLANE > me)
        def _():
            plane_copy(1, step, True).start()

        return carry

    lax.fori_loop(1, PLANE, send_own, 0)

    weight_copies = [
        remote(src.at[0], dst.at[tp], weight_send.at[i], weight_got.at[i], (sp, other))
        for i, (src, dst) in enumerate(((gate_hbm, gate_w), (up_hbm, up_w), (down_hbm, down_w)))
    ]
    for copy in weight_copies:
        copy.start()

    lane = lax.broadcasted_iota(jnp.int32, (ROWS, 128), 1)
    low_lanes = lane < 64

    def attend(first, second, causal):
        rows = jnp.concatenate([first[:HALF, :], second[:HALF, :]], axis=0)
        low, high = [], []
        for half in (first, second):
            extra = half[HALF:PIECE, :].astype(jnp.float32)
            for tile in (extra[:, :128], extra[:, 128:]):
                swapped = pltpu.roll(tile, 64, 1)
                low += [tile, swapped]
                high += [swapped, tile]
        low = jnp.concatenate(low, axis=0).astype(jnp.bfloat16)
        high = jnp.concatenate(high, axis=0).astype(jnp.bfloat16)
        keys = nn(rows, key_w_ref[...]).astype(jnp.bfloat16)
        values = nt(value_w_ref[...], rows).astype(jnp.bfloat16)
        for head in range(HEADS):
            column = keys[:, 128 * (head // 2) : 128 * (head // 2) + 128]
            if head % 2 == 0:
                full_key = jnp.where(low_lanes, column, high)
            else:
                full_key = jnp.where(low_lanes, low, column)
            scores = nn(full_key, query_ref[head])
            if causal:
                key_at = lax.broadcasted_iota(jnp.int32, (ROWS, ROWS), 0)
                query_at = lax.broadcasted_iota(jnp.int32, (ROWS, ROWS), 1)
                scores = jnp.where(key_at <= query_at, scores, -MASKED)
                new_max = jnp.max(scores, axis=0, keepdims=True)
            else:
                old_max = run_max[head]
                new_max = jnp.maximum(old_max, jnp.max(scores, axis=0, keepdims=True))
            weights = jnp.exp2((scores - new_max) * SCORE_BASE2)
            sums = jnp.sum(weights.reshape(ROWS // 8, 8, ROWS), axis=0)
            part = nn(values[64 * head : 64 * head + 64, :], weights.astype(jnp.bfloat16))
            if causal:
                run_sum[head] = sums
                run_out[head] = part
            else:
                factor = jnp.exp2((old_max - new_max) * SCORE_BASE2)
                run_sum[head] = run_sum[head] * factor + sums
                run_out[head] = run_out[head] * factor + part
            run_max[head] = new_max

    attend(own_ref.at[0], own_ref.at[1], True)

    def pass_copy(kind, source):
        return remote(
            kv.at[kind, source, tp],
            kv.at[kind, source, tp],
            pass_send.at[kind, source],
            passed.at[kind, source],
            (sp, other),
        )

    def arrival(kind, source):
        return pltpu.make_async_copy(
            kv.at[kind, source, tp], kv.at[kind, source, tp], got.at[kind, source]
        )

    arrival(0, me).wait()
    pass_copy(0, me).start()

    def send_first(step, carry):
        plane_copy(0, step, False).start()
        return carry

    lax.fori_loop(1, PLANE, send_first, 0)
    arrival(1, me).wait()
    pass_copy(1, me).start()

    def send_second(step, carry):
        @pl.when((me + step) % PLANE < me)
        def _():
            plane_copy(1, step, False).start()

        return carry

    lax.fori_loop(1, PLANE, send_second, 0)

    def visit(number, carry):
        step = number // 2
        kind = number % 2
        source = (me - step + PLANE) % PLANE

        later = number + 2

        @pl.when(later < 2 * PLANE)
        def _():
            later_source = (me - later // 2 + PLANE) % PLANE
            arrival(kind, later_source).wait()
            pass_copy(kind, later_source).start()

        pltpu.make_async_copy(
            kv.at[kind, source, other], kv.at[kind, source, other], passed.at[kind, source]
        ).wait()
        live = jnp.where(kind == 0, (z >= 1).astype(jnp.int32), ((source < me) | (z >= 2)).astype(jnp.int32))

        @pl.when(live == 1)
        def _():
            attend(kv.at[kind, source, 0], kv.at[kind, source, 1], False)

        return carry

    lax.fori_loop(0, 2 * PLANE, visit, 0)

    for head in range(HEADS):
        total = jnp.sum(run_sum[head], axis=0, keepdims=True)
        done = (run_out[head] / total).astype(jnp.bfloat16)
        for part in range(2):
            turned_out[part, 64 * head : 64 * head + 64, :] = done[:, HALF * part : HALF * part + HALF]
    heads_copy = remote(
        turned_out.at[other], heads_buf.at[tp], heads_send, heads_got, (sp, other)
    )
    heads_copy.start()
    heads_buf[tp] = turned_out[tp]
    local_copies[0].wait()
    heads_copy.wait_recv()

    attended = jnp.concatenate(
        [heads_buf[g].astype(jnp.float32).T.astype(jnp.bfloat16) for g in range(2)], axis=1
    )
    squares = jnp.zeros((HALF, 1), jnp.float32)
    for n in range(4):
        cols = slice(512 * n, 512 * n + 512)
        part = nn(attended, proj[:, cols])
        mix[:, cols] = part
        squares = squares + jnp.sum(part * part, axis=1, keepdims=True)
    scale = lax.rsqrt(squares * (1.0 / D) + epsilon)
    squares = jnp.zeros((HALF, 1), jnp.float32)
    for n in range(4):
        cols = slice(512 * n, 512 * n + 512)
        branch = mix[:, cols] * scale * mix_gain_ref[:, cols]
        mid = (residual_ref[:, cols].astype(jnp.float32) + branch).astype(jnp.bfloat16)
        middle[:, cols] = mid
        wide = mid.astype(jnp.float32)
        squares = squares + jnp.sum(wide * wide, axis=1, keepdims=True)
    scale = lax.rsqrt(squares * (1.0 / D) + epsilon)
    for n in range(4):
        cols = slice(512 * n, 512 * n + 512)
        normed[:, cols] = (
            middle[:, cols].astype(jnp.float32) * scale * moe_gain_ref[:, cols]
        ).astype(jnp.bfloat16)

    at_row = lax.broadcasted_iota(jnp.int32, (HALF, HALF), 0)
    at_col = lax.broadcasted_iota(jnp.int32, (HALF, HALF), 1)
    expert_row = lax.broadcasted_iota(jnp.int32, (EXPERTS, HALF), 0)
    hot = [(expert_row == ids_t_ref[k : k + 1, :]).astype(jnp.float32) for k in range(2)]
    earlier = nn(
        (hot[0] + hot[1]).astype(jnp.bfloat16), (at_row < at_col).astype(jnp.float32).astype(jnp.bfloat16)
    )
    slot_row = lax.broadcasted_iota(jnp.int32, (EXPERTS * CAP, HALF), 0)
    chooser = jnp.zeros((EXPERTS * CAP, HALF), jnp.float32)
    for k in range(2):
        rank = jnp.sum(hot[k] * earlier, axis=0, keepdims=True).astype(jnp.int32)
        slot = ids_t_ref[k : k + 1, :] * CAP + rank
        chooser = chooser + (slot_row == slot).astype(jnp.float32)
    chooser = chooser.astype(jnp.bfloat16)
    for n in range(8):
        cols = slice(256 * n, 256 * n + 256)
        picked = nn(chooser, normed[:, cols]).astype(jnp.bfloat16)
        send_buf[:, :, cols] = picked.reshape(EXPERTS, CAP, 256)

    def go_copy(step):
        target = (sp + step) % EXPERTS
        return remote(
            send_buf.at[target], recv_buf.at[sp], go_send.at[step], go_got.at[sp], (target, tp)
        )

    def go(step, carry):
        go_copy(step).start()
        return carry

    lax.fori_loop(1, EXPERTS, go, 0)
    mine = pltpu.make_async_copy(send_buf.at[sp], recv_buf.at[sp], own_copy)
    mine.start()
    for copy in local_copies[1:]:
        copy.wait()
    for copy in weight_copies:
        copy.wait_recv()
    mine.wait()

    def back_copy(source):
        return remote(
            done_buf.at[source], back_buf.at[sp], back_send.at[source], back_got.at[sp], (source, tp)
        )

    def expert_group(number, carry):
        group = (z - number + DEPTH) % DEPTH
        first = group * PLANE

        def await_rows(i, c):
            source = first + i

            @pl.when(source != sp)
            def _():
                pltpu.make_async_copy(
                    recv_buf.at[source], recv_buf.at[source], go_got.at[source]
                ).wait()

            return c

        lax.fori_loop(0, PLANE, await_rows, 0)
        rows = recv_buf[pl.ds(first, PLANE)].reshape(PLANE * CAP, D)
        hidden = []
        for half in range(2):
            gate_out = nn(rows, gate_w[half])
            up_out = nn(rows, up_w[half])
            hidden.append((gate_out / (1.0 + jnp.exp(-gate_out)) * up_out).astype(jnp.bfloat16))
        for n in range(4):
            cols = slice(512 * n, 512 * n + 512)
            parts = [
                nn(hidden[half], down_w[half, :, cols]).astype(jnp.bfloat16).astype(jnp.float32)
                for half in range(2)
            ]
            done_buf[pl.ds(first, PLANE), :, cols] = (
                (parts[0] + parts[1]).astype(jnp.bfloat16).reshape(PLANE, CAP, 512)
            )

        def send_back(i, c):
            source = first + i

            @pl.when(source != sp)
            def _():
                back_copy(source).start()

            return c

        lax.fori_loop(0, PLANE, send_back, 0)
        return carry

    lax.fori_loop(0, DEPTH, expert_group, 0)
    mine_back = pltpu.make_async_copy(done_buf.at[sp], back_buf.at[sp], own_copy)
    mine_back.start()

    expert_col = lax.broadcasted_iota(jnp.int32, (HALF, EXPERTS), 1)
    hot = [(expert_col == ids_ref[:, k : k + 1]).astype(jnp.float32) for k in range(2)]
    earlier = nn(
        (at_col < at_row).astype(jnp.float32).astype(jnp.bfloat16), (hot[0] + hot[1]).astype(jnp.bfloat16)
    )
    slot_col = lax.broadcasted_iota(jnp.int32, (HALF, EXPERTS * CAP), 1)
    takers = []
    for k in range(2):
        rank = jnp.sum(hot[k] * earlier, axis=1, keepdims=True).astype(jnp.int32)
        slot = ids_ref[:, k : k + 1] * CAP + rank
        takers.append((slot_col == slot).astype(jnp.float32).astype(jnp.bfloat16))

    mine_back.wait()

    def await_back(step, carry):
        source = (sp + step) % EXPERTS
        pltpu.make_async_copy(
            back_buf.at[source], back_buf.at[source], back_got.at[source]
        ).wait()
        return carry

    lax.fori_loop(1, EXPERTS, await_back, 0)
    for n in range(4):
        cols = slice(512 * n, 512 * n + 512)
        came = back_buf[:, :, cols].reshape(EXPERTS * CAP, 512)
        both = (
            nn(takers[0], came) * route_ref[:, 0:1] + nn(takers[1], came) * route_ref[:, 1:2]
        )
        out_ref[:, cols] = (middle[:, cols].astype(jnp.float32) + both).astype(jnp.bfloat16)

    for copy in next_z:
        copy.wait_send()
    for copy in weight_copies:
        copy.wait_send()
    heads_copy.wait_send()

    def plane_done(step, carry):
        plane_copy(0, step, True).wait_send()
        plane_copy(1, step, True).wait_send()
        return carry

    lax.fori_loop(1, PLANE, plane_done, 0)

    def pass_done(source, carry):
        pass_copy(0, source).wait_send()
        pass_copy(1, source).wait_send()
        return carry

    lax.fori_loop(0, PLANE, pass_done, 0)

    def moe_done(step, carry):
        go_copy(step).wait_send()
        back_copy((sp + step) % EXPERTS).wait_send()
        return carry

    lax.fori_loop(1, EXPERTS, moe_done, 0)


def local(
    residual,
    queries,
    latent,
    rope_key,
    doc_ids,
    latent_to_key,
    latent_to_value,
    out_proj,
    mix_gain,
    moe_gain,
    expert_ids,
    route_weight,
    gate_weight,
    up_weight,
    down_weight,
):
    bf16, f32 = jnp.bfloat16, jnp.float32
    first = lax.axis_index("sp") * ROWS
    positions = (first + jnp.arange(ROWS, dtype=jnp.int32)).astype(f32)
    half_width = ROPE // 2
    frequency = rope_base ** (-jnp.arange(half_width, dtype=f32) / half_width)
    angles = positions[:, None] * frequency[None, :]
    cosine, sine_part = jnp.cos(angles), jnp.sin(angles)
    hot = (doc_ids[:, None] == jnp.arange(8, dtype=jnp.int32)[None, :]).astype(f32)
    key_extra = jnp.concatenate(
        [rotate(rope_key, cosine, sine_part), hot.astype(bf16), jnp.zeros((ROWS, 24), bf16)], axis=1
    )
    key_extra = (
        key_extra.reshape(2, 4, 32, 64).transpose(0, 2, 1, 3).reshape(2, PIECE - HALF, LATENT)
    )
    own = jnp.concatenate([latent.reshape(2, HALF, LATENT), key_extra], axis=1)
    shaped = queries.reshape(ROWS, HEADS, UNROTATED_DIM + ROPE)
    plain = shaped[..., :UNROTATED_DIM]
    turned = rotate(shaped[..., UNROTATED_DIM:], cosine[:, None, :], sine_part[:, None, :])
    mask = jnp.broadcast_to(((hot - 1.0) * MASKED).astype(bf16)[:, None, :], (ROWS, HEADS, 8))
    extra = jnp.concatenate([turned, mask, jnp.zeros((ROWS, HEADS, 24), bf16)], axis=2)
    even = jnp.concatenate([plain[:, 0::2], extra[:, 0::2]], axis=2)
    odd = jnp.concatenate([extra[:, 1::2], plain[:, 1::2]], axis=2)
    query = jnp.stack([even, odd], axis=2).reshape(ROWS, HEADS, 128).transpose(1, 2, 0)

    vmem = pl.BlockSpec(memory_space=pltpu.VMEM)
    anywhere = pl.BlockSpec(memory_space=pl.ANY)
    dma = pltpu.SemaphoreType.DMA
    return pl.pallas_call(
        kernel,
        out_shape=jax.ShapeDtypeStruct((HALF, D), bf16),
        in_specs=[vmem] * 10 + [anywhere] * 4,
        out_specs=vmem,
        scratch_shapes=[
            pltpu.VMEM((2, PLANE, 2, PIECE, LATENT), bf16),
            pltpu.VMEM((HEADS, 1, ROWS), f32),
            pltpu.VMEM((HEADS, 8, ROWS), f32),
            pltpu.VMEM((HEADS, 64, ROWS), f32),
            pltpu.VMEM((2, HEADS * 64, HALF), bf16),
            pltpu.VMEM((2, HEADS * 64, HALF), bf16),
            pltpu.VMEM((2 * HEADS * 64, D), bf16),
            pltpu.VMEM((2, D, FF_HALF), bf16),
            pltpu.VMEM((2, D, FF_HALF), bf16),
            pltpu.VMEM((2, FF_HALF, D), bf16),
            pltpu.VMEM((HALF, D), f32),
            pltpu.VMEM((HALF, D), bf16),
            pltpu.VMEM((HALF, D), bf16),
            pltpu.VMEM((EXPERTS, CAP, D), bf16),
            pltpu.VMEM((EXPERTS, CAP, D), bf16),
            pltpu.VMEM((EXPERTS, CAP, D), bf16),
            pltpu.VMEM((EXPERTS, CAP, D), bf16),
            dma((2,)),
            dma((2, PLANE)),
            dma((2, PLANE)),
            dma((2, PLANE)),
            dma((2, PLANE)),
            dma((4,)),
            dma((3,)),
            dma((3,)),
            dma,
            dma,
            dma((EXPERTS,)),
            dma((EXPERTS,)),
            dma,
            dma((EXPERTS,)),
            dma((EXPERTS,)),
        ],
        compiler_params=pltpu.CompilerParams(
            collective_id=0, has_side_effects=True, vmem_limit_bytes=60 * 1024 * 1024
        ),
    )(
        query,
        own,
        latent_to_key,
        latent_to_value.T,
        residual,
        mix_gain.reshape(1, D),
        moe_gain.reshape(1, D),
        expert_ids,
        expert_ids.T,
        route_weight,
        out_proj,
        gate_weight,
        up_weight,
        down_weight,
    )


def solution(mesh):
    in_specs = (
        P(("sp", "tp"), None),
        P("sp", "tp"),
        P("sp", None),
        P("sp", None),
        P("sp"),
        P(None, "tp"),
        P(None, "tp"),
        P(),
        P(),
        P(),
        P(("sp", "tp"), None),
        P(("sp", "tp"), None),
        P("sp", None, "tp"),
        P("sp", None, "tp"),
        P("sp", "tp", None),
    )
    out_specs = P(("sp", "tp"), None)
    return jax.shard_map(local, mesh=mesh, in_specs=in_specs, out_specs=out_specs, check_vma=False)
```

time: 649 us -> 175 us (0.27); the launches traced: 637 us -> 173 us
  blocking collectives: 332 us -> 0 us
  Pallas kernels: 0 us -> 161 us
  local copies, waits for them, and re-layouts: 160 us -> 7.05 us
  loops' own time: 64.4 us -> 0 us
  waiting for transfers between devices: 29.2 us -> 0 us
  matrix products: 14.5 us -> 0 us
  between operations: 13.7 us -> 0.11 us
  other arithmetic: 17 us -> 5.2 us
    all_to_all x4 -> x0, blocking collectives: 173 us -> none  [the longest x1 123 us: local(): lax.all_to_all(buffer, 'sp', split_axis=0, concat_axis=0, tiled=True)]
    pallas_call x0 -> x1, Pallas kernels: none -> 161 us  [local(): pl.pallas_call(kernel, out_shape=jax.ShapeDtypeStruct((HALF, D), bf16), i...]
    all_gather x1 -> x0, blocking collectives: 159 us -> none  [local(): lax.all_gather(doc_ids, 'sp', axis=0, tiled=True)]
    slice x97 -> x3, local copies, waits for them, and re-layouts: 104 us -> 0.04 us  [the longest x2 0.03 us: local(): even = jnp.concatenate([plain[:, 0::2], extra[:, 0::2]], axis=2)]
    another operation x33 -> x0, loops' own time: 64.4 us -> none  [the longest x1 63.9 us: local(): running = lax.fori_loop(0, row_count // block_rows, one_block, initial)]
    all_to_all x1 -> x0, waiting for transfers between devices: 28.5 us -> none  [local(): lax.all_to_all(summed, 'sp', split_axis=0, concat_axis=0, tiled=True)]
    dynamic_slice x32 -> x0, local copies, waits for them, and re-layouts: 24.2 us -> none  [one_block(): lax.dynamic_slice_in_dim(member, first_row, block_rows, 0)]
    iota x32 -> x0, local copies, waits for them, and re-layouts: 19.1 us -> none  [one_block(): key_pos = first_row + jnp.arange(block_rows, dtype=jnp.int32)]
  transfers between devices with their start and end apart: 3 -> 0, of which waited for: 1 -> 0; matrix products, arithmetic and copies ran while one was open for 1% -> 0% of each run, Pallas kernels for 0% -> 0%
where the time goes in v1:
time: 175 us; the launch traced here: 173 us
  Pallas kernels  161 us (92%)
  local copies, waits for them, and re-layouts  7.05 us (4%)
  other arithmetic  5.2 us (3%)
    pallas_call x1, Pallas kernels, local(): pl.pallas_call(kernel, out_shape=jax.ShapeDtypeStruct((HALF, D), bf16), i...  161 us
    unnamed x8, local copies, waits for them, and re-layouts  5.53 us

profile of v1, /device:TPU:1, one launch (start us, length us, event | category | flops | bytes accessed | tf_op | source)
XLA Modules:
  0.0 172.9 jit_solution(11886090819828559488)
XLA Ops:
  0.0 0.1 pad.15.clone
  0.1 0.8 eq.29
  0.9 0.7 multiply_convert_fusion
  1.6 0.1 copy.23
  1.7 0.1 convert_convert_fusion
  1.8 0.9 fusion.5
  2.7 0.1 concatenate.30
  2.8 0.1 copy.24
  2.9 0.1 concatenate.31
  3.0 0.0 copy-start.1
  3.0 0.1 copy.25
  3.1 0.2 maximum_bitcast_fusion.2
  3.3 0.1 reshape.115
  3.4 1.4 copy.28.route_ref
  4.8 1.4 copy.27.ids_ref
  6.2 0.9 fusion.1
  7.1 0.1 maximum_maximum_fusion
  7.2 1.6 pad_maximum_fusion.1.own_ref
  8.8 0.0 copy-done
  8.9 0.8 pad_maximum_fusion
  9.7 0.0 copy-done.1
  9.7 0.8 copy.26
  10.5 160.6 %shard_map.145 = bf16[128,2048]{1,0:T(8,128)(2,1)} custom-call(bf16[6,128,256]{2,1,0:T(8,128)(2,1)} %bitcast.21, bf16[2,160,256]{2,1,0:T(8,128)(2,1)} %pad_maximum_fusion.1.own_ref, bf16[256,384]{1,0:T(8,128)(2,1)} %key_w_ref.1, bf16[384,256]{1,0:T(8,128)(2,1)} %bitcast.22, bf16[128,2048]{1,0:T(8,128)(2,1)} %residual_ref.1, f32[1,2048]{1,0:T(1,128)} %bitcast.26, ...), custom_call_target="tpu_custom_call" | custom-call | tf_op jit(solution)/shard_map/pallas_call | solution.py:514
  171.1 1.9 %copy.30 = bf16[128,2048]{1,0:T(8,128)(2,1)} copy(bf16[128,2048]{1,0:T(8,128)(2,1)} %shard_map.145) | data formatting | bytes 1048576
  (9 shorter events, 0.1 us)
Async XLA Ops:
  0.0 8.8 %copy-start = (bf16[256,576]{0,1:T(8,128)(2,1)S(1)}, bf16[256,576]{0,1:T(8,128)(2,1)}, u32[]{:S(2)}) copy-start(bf16[256,576]{0,1:T(8,128)(2,1)} %param.16) | copy-start | bytes 884740
  3.0 6.7 %copy-start.1 = (bf16[256,384]{1,0:T(8,128)(2,1)S(1)}, bf16[256,384]{1,0:T(8,128)(2,1)}, u32[]{:S(2)}) copy-start(bf16[256,384]{1,0:T(8,128)(2,1)} %param.21) | copy-start | bytes 589828

commit v2 on v1

--- a/solution.py
+++ b/solution.py
@@ -20,11 +20,46 @@
 FF_HALF = 512
 PLANE = 16
 DEPTH = 4
+GROUP = 2
+GROUPS = HEADS // GROUP
+CHUNK = 64
+STEP = 4 * ROWS
+DEAD = 40
 rope_base = 10000.0
 epsilon = 1e-06
 MASKED = 1e30
 SCORE_BASE2 = float((UNROTATED_DIM + ROPE) ** (-0.5) * 1.4426950408889634)
 MESH = pl.DeviceIdType.MESH
+
+
+def hops(offset):
+    return [min(v, DEPTH - v) for v in offset]
+
+
+def exchange_order():
+    cube = [(a, b, c) for a in range(DEPTH) for b in range(DEPTH) for c in range(DEPTH)]
+    classes = []
+    for kind in range(DEPTH):
+        left = [o for o in cube if sum(o) % DEPTH == kind and any(o)]
+        order, load = [], [0, 0, 0]
+        while left:
+            best = min(
+                left,
+                key=lambda o: (
+                    max(a + b for a, b in zip(load, hops(o))) - min(a + b for a, b in zip(load, hops(o))),
+                    -sum(hops(o)),
+                    o,
+                ),
+            )
+            left.remove(best)
+            order.append(best)
+            load = [a + b for a, b in zip(load, hops(best))]
+        classes.append(order if kind else order + [(0, 0, 0)])
+    return classes
+
+
+ORDER = exchange_order()
+OWN_SLOT = PLANE - 1
 
 
 def rotate(source, cosine, sine_part):
@@ -67,7 +102,12 @@
     out_ref,
     kv,
     run_max,
-    run_sum,
+    held,
+    tops,
+    factors,
+    probs,
+    full_keys,
+    values,
     run_out,
     turned_out,
     heads_buf,
@@ -175,50 +215,85 @@
     for copy in weight_copies:
         copy.start()
 
-    lane = lax.broadcasted_iota(jnp.int32, (ROWS, 128), 1)
-    low_lanes = lane < 64
-
-    def attend(first, second, causal):
-        rows = jnp.concatenate([first[:HALF, :], second[:HALF, :]], axis=0)
-        low, high = [], []
-        for half in (first, second):
-            extra = half[HALF:PIECE, :].astype(jnp.float32)
-            for tile in (extra[:, :128], extra[:, 128:]):
-                swapped = pltpu.roll(tile, 64, 1)
-                low += [tile, swapped]
-                high += [swapped, tile]
-        low = jnp.concatenate(low, axis=0).astype(jnp.bfloat16)
-        high = jnp.concatenate(high, axis=0).astype(jnp.bfloat16)
-        keys = nn(rows, key_w_ref[...]).astype(jnp.bfloat16)
-        values = nt(value_w_ref[...], rows).astype(jnp.bfloat16)
-        for head in range(HEADS):
-            column = keys[:, 128 * (head // 2) : 128 * (head // 2) + 128]
-            if head % 2 == 0:
-                full_key = jnp.where(low_lanes, column, high)
-            else:
-                full_key = jnp.where(low_lanes, low, column)
-            scores = nn(full_key, query_ref[head])
+    values[...] = jnp.ones_like(values)
+    low_lanes = lax.broadcasted_iota(jnp.int32, (HALF, 128), 1) < 64
+    dead_lane = (lax.broadcasted_iota(jnp.int32, (PIECE - HALF, 128), 1) % 64 == DEAD).astype(
+        jnp.float32
+    )
+
+    def project(blocks, dead, bank):
+        for number, (block, flag) in enumerate(zip(blocks, dead)):
+            at = ROWS * number
+            for half in range(2):
+                low, high = [], []
+                for tile in range(2):
+                    extra = block[half, HALF:PIECE, 128 * tile : 128 * tile + 128].astype(jnp.float32)
+                    if flag is not None:
+                        extra = extra + dead_lane * flag
+                    swapped = pltpu.roll(extra, 64, 1)
+                    low += [extra, swapped]
+                    high += [swapped, extra]
+                low = jnp.concatenate(low, axis=0).astype(jnp.bfloat16)
+                high = jnp.concatenate(high, axis=0).astype(jnp.bfloat16)
+                keys = nn(block[half, :HALF, :], key_w_ref[...]).astype(jnp.bfloat16)
+                for head in range(HEADS):
+                    column = keys[:, 128 * (head // 2) : 128 * (head // 2) + 128]
+                    if head % 2 == 0:
+                        full_key = jnp.where(low_lanes, column, high)
+                    else:
+                        full_key = jnp.where(low_lanes, low, column)
+                    full_keys[head, at + HALF * half : at + HALF * half + HALF, :] = full_key
+            rows = jnp.concatenate([block[0, :HALF, :], block[1, :HALF, :]], axis=0)
+            every = nt(value_w_ref[...], rows).astype(jnp.bfloat16)
+            for head in range(HEADS):
+                values[bank, head, :64, at : at + ROWS] = every[64 * head : 64 * head + 64, :]
+
+    def score(first, slot, keys_at, causal):
+        for i in range(GROUP):
+            head = first + i
+            top = None
+            for number in range(keys_at // HALF):
+                at = HALF * number
+                scores = nn(full_keys[head, at : at + HALF, :], query_ref[head])
+                if causal:
+                    key_at = lax.broadcasted_iota(jnp.int32, (HALF, ROWS), 0) + at
+                    query_at = lax.broadcasted_iota(jnp.int32, (HALF, ROWS), 1)
+                    scores = jnp.where(key_at <= query_at, scores, -MASKED)
+                held[slot, i, at : at + HALF, :] = scores
+                here = jnp.max(scores.reshape(HALF // 8, 8, ROWS), axis=0)
+                top = here if top is None else jnp.maximum(top, here)
+            tops[slot, i] = jnp.max(top, axis=0, keepdims=True)
+
+    def weigh(first, slot, keys_at, causal):
+        for i in range(GROUP):
+            head = first + i
             if causal:
-                key_at = lax.broadcasted_iota(jnp.int32, (ROWS, ROWS), 0)
-                query_at = lax.broadcasted_iota(jnp.int32, (ROWS, ROWS), 1)
-                scores = jnp.where(key_at <= query_at, scores, -MASKED)
-                new_max = jnp.max(scores, axis=0, keepdims=True)
+                new_max = tops[slot, i]
             else:
                 old_max = run_max[head]
-                new_max = jnp.maximum(old_max, jnp.max(scores, axis=0, keepdims=True))
-            weights = jnp.exp2((scores - new_max) * SCORE_BASE2)
-            sums = jnp.sum(weights.reshape(ROWS // 8, 8, ROWS), axis=0)
-            part = nn(values[64 * head : 64 * head + 64, :], weights.astype(jnp.bfloat16))
+                new_max = jnp.maximum(old_max, tops[slot, i])
+                factors[head] = jnp.exp2((old_max - new_max) * SCORE_BASE2)
+            run_max[head] = new_max
+            for number in range(keys_at // CHUNK):
+                at = CHUNK * number
+                probs[slot, i, at : at + CHUNK, :] = jnp.exp2(
+                    (held[slot, i, at : at + CHUNK, :] - new_max) * SCORE_BASE2
+                ).astype(jnp.bfloat16)
+
+    def gather_values(first, slot, keys_at, bank, causal):
+        for i in range(GROUP):
+            head = first + i
+            part = nn(values[bank, head, :, :keys_at], probs[slot, i, :keys_at, :])
             if causal:
-                run_sum[head] = sums
                 run_out[head] = part
             else:
-                factor = jnp.exp2((old_max - new_max) * SCORE_BASE2)
-                run_sum[head] = run_sum[head] * factor + sums
-                run_out[head] = run_out[head] * factor + part
-            run_max[head] = new_max
-
-    attend(own_ref.at[0], own_ref.at[1], True)
+                run_out[head] = run_out[head] * factors[head] + part
+
+    project([own_ref], [None], 1)
+    for j in range(GROUPS):
+        score(j * GROUP, j % 2, ROWS, True)
+        weigh(j * GROUP, j % 2, ROWS, True)
+        gather_values(j * GROUP, j % 2, ROWS, 1, True)
 
     def pass_copy(kind, source):
         return remote(
@@ -253,36 +328,65 @@
         return carry
 
     lax.fori_loop(1, PLANE, send_second, 0)
-
-    def visit(number, carry):
-        step = number // 2
-        kind = number % 2
-        source = (me - step + PLANE) % PLANE
-
-        later = number + 2
-
-        @pl.when(later < 2 * PLANE)
+    before = (me - 1 + PLANE) % PLANE
+    for kind in range(2):
+        arrival(kind, before).wait()
+        pass_copy(kind, before).start()
+
+    steps = jnp.where(z >= 1, PLANE // 2, me // 2 + 1)
+    last_slot = (GROUPS - 1) % 2
+    last_head = (GROUPS - 1) * GROUP
+
+    def visit(step, carry):
+        sources = [(me - 2 * step - i + PLANE) % PLANE for i in range(2)]
+
+        @pl.when(step < PLANE // 2 - 1)
         def _():
-            later_source = (me - later // 2 + PLANE) % PLANE
-            arrival(kind, later_source).wait()
-            pass_copy(kind, later_source).start()
-
-        pltpu.make_async_copy(
-            kv.at[kind, source, other], kv.at[kind, source, other], passed.at[kind, source]
-        ).wait()
-        live = jnp.where(kind == 0, (z >= 1).astype(jnp.int32), ((source < me) | (z >= 2)).astype(jnp.int32))
-
-        @pl.when(live == 1)
+            for i in range(2):
+                later = (me - 2 * step - 2 - i + PLANE) % PLANE
+                for kind in range(2):
+                    arrival(kind, later).wait()
+                    pass_copy(kind, later).start()
+
+        for source in sources:
+            for kind in range(2):
+                pltpu.make_async_copy(
+                    kv.at[kind, source, other], kv.at[kind, source, other], passed.at[kind, source]
+                ).wait()
+
+        @pl.when(step < steps)
         def _():
-            attend(kv.at[kind, source, 0], kv.at[kind, source, 1], False)
-
-        return carry
-
-    lax.fori_loop(0, 2 * PLANE, visit, 0)
+            bank = step % 2
+            blocks, dead = [], []
+            for source in sources:
+                blocks += [kv.at[0, source], kv.at[1, source]]
+                dead += [
+                    (z < 1).astype(jnp.float32),
+                    ((source >= me) & (z < 2)).astype(jnp.float32),
+                ]
+
+            project(blocks, dead, bank)
+            score(0, 0, STEP, False)
+
+            for j in range(GROUPS - 1):
+
+                @pl.when(step >= -1 - j)
+                def _(j=j):
+                    if j > 0:
+                        gather_values((j - 1) * GROUP, (j - 1) % 2, STEP, bank, False)
+                    weigh(j * GROUP, j % 2, STEP, False)
+                    score((j + 1) * GROUP, (j + 1) % 2, STEP, False)
+
+            gather_values(last_head - GROUP, (last_slot + 1) % 2, STEP, bank, False)
+            weigh(last_head, last_slot, STEP, False)
+            gather_values(last_head, last_slot, STEP, bank, False)
+
+        return carry
+
+    lax.fori_loop(0, PLANE // 2, visit, 0)
 
     for head in range(HEADS):
-        total = jnp.sum(run_sum[head], axis=0, keepdims=True)
-        done = (run_out[head] / total).astype(jnp.bfloat16)
+        done = (run_out[head, :64, :] / run_out[head, 64:65, :]).astype(jnp.bfloat16)
         for part in range(2):
             turned_out[part, 64 * head : 64 * head + 64, :] = done[:, HALF * part : HALF * part + HALF]
     heads_copy = remote(
@@ -337,18 +441,34 @@
         picked = nn(chooser, normed[:, cols]).astype(jnp.bfloat16)
         send_buf[:, :, cols] = picked.reshape(EXPERTS, CAP, 256)
 
-    def go_copy(step):
-        target = (sp + step) % EXPERTS
+    y, x = me // DEPTH, me % DEPTH
+
+    def toward(offset, sign):
+        dz, dy, dx = offset
+        return (
+            ((z + sign * dz + DEPTH) % DEPTH) * PLANE
+            + ((y + sign * dy + DEPTH) % DEPTH) * DEPTH
+            + (x + sign * dx + DEPTH) % DEPTH
+        )
+
+    def go_copy(kind, i):
+        target = toward(ORDER[kind][i], 1)
+        slot = kind * PLANE + i
         return remote(
-            send_buf.at[target], recv_buf.at[sp], go_send.at[step], go_got.at[sp], (target, tp)
-        )
-
-    def go(step, carry):
-        go_copy(step).start()
-        return carry
-
-    lax.fori_loop(1, EXPERTS, go, 0)
-    mine = pltpu.make_async_copy(send_buf.at[sp], recv_buf.at[sp], own_copy)
+            send_buf.at[target], recv_buf.at[slot], go_send.at[slot], go_got.at[slot], (target, tp)
+        )
+
+    def back_copy(kind, i):
+        source = toward(ORDER[kind][i], -1)
+        slot = kind * PLANE + i
+        return remote(
+            done_buf.at[slot], back_buf.at[sp], back_send.at[slot], back_got.at[sp], (source, tp)
+        )
+
+    away = [(kind, i) for kind in range(DEPTH) for i in range(PLANE) if any(ORDER[kind][i])]
+    for kind, i in away:
+        go_copy(kind, i).start()
+    mine = pltpu.make_async_copy(send_buf.at[sp], recv_buf.at[OWN_SLOT], own_copy)
     mine.start()
     for copy in local_copies[1:]:
         copy.wait()
@@ -356,27 +476,8 @@
         copy.wait_recv()
     mine.wait()
 
-    def back_copy(source):
-        return remote(
-            done_buf.at[source], back_buf.at[sp], back_send.at[source], back_got.at[sp], (source, tp)
-        )
-
-    def expert_group(number, carry):
-        group = (z - number + DEPTH) % DEPTH
-        first = group * PLANE
-
-        def await_rows(i, c):
-            source = first + i
-
-            @pl.when(source != sp)
-            def _():
-                pltpu.make_async_copy(
-                    recv_buf.at[source], recv_buf.at[source], go_got.at[source]
-                ).wait()
-
-            return c
-
-        lax.fori_loop(0, PLANE, await_rows, 0)
+    def expert_group(kind, carry):
+        first = kind * PLANE
         rows = recv_buf[pl.ds(first, PLANE)].reshape(PLANE * CAP, D)
         hidden = []
         for half in range(2):
@@ -393,20 +494,31 @@
                 (parts[0] + parts[1]).astype(jnp.bfloat16).reshape(PLANE, CAP, 512)
             )
 
-        def send_back(i, c):
-            source = first + i
-
-            @pl.when(source != sp)
-            def _():
-                back_copy(source).start()
-
-            return c
-
-        lax.fori_loop(0, PLANE, send_back, 0)
-        return carry
-
-    lax.fori_loop(0, DEPTH, expert_group, 0)
-    mine_back = pltpu.make_async_copy(done_buf.at[sp], back_buf.at[sp], own_copy)
+    def turn(kind, carry):
+        for k in range(DEPTH):
+
+            @pl.when(kind == k)
+            def _(k=k):
+                for i in range(PLANE):
+                    if any(ORDER[k][i]):
+                        slot = k * PLANE + i
+                        pltpu.make_async_copy(
+                            recv_buf.at[slot], recv_buf.at[slot], go_got.at[slot]
+                        ).wait()
+
+        expert_group(kind, carry)
+        for k in range(DEPTH):
+
+            @pl.when(kind == k)
+            def _(k=k):
+                for i in range(PLANE):
+                    if any(ORDER[k][i]):
+                        back_copy(k, i).start()
+
+        return carry
+
+    lax.fori_loop(0, DEPTH, turn, 0)
+    mine_back = pltpu.make_async_copy(done_buf.at[OWN_SLOT], back_buf.at[sp], own_copy)
     mine_back.start()
 
     expert_col = lax.broadcasted_iota(jnp.int32, (HALF, EXPERTS), 1)
@@ -459,12 +571,9 @@
 
     lax.fori_loop(0, PLANE, pass_done, 0)
 
-    def moe_done(step, carry):
-        go_copy(step).wait_send()
-        back_copy((sp + step) % EXPERTS).wait_send()
-        return carry
-
-    lax.fori_loop(1, EXPERTS, moe_done, 0)
+    for kind, i in away:
+        go_copy(kind, i).wait_send()
+        back_copy(kind, i).wait_send()
 
 
 def local(
@@ -503,7 +612,7 @@
     plain = shaped[..., :UNROTATED_DIM]
     turned = rotate(shaped[..., UNROTATED_DIM:], cosine[:, None, :], sine_part[:, None, :])
     mask = jnp.broadcast_to(((hot - 1.0) * MASKED).astype(bf16)[:, None, :], (ROWS, HEADS, 8))
-    extra = jnp.concatenate([turned, mask, jnp.zeros((ROWS, HEADS, 24), bf16)], axis=2)
+    extra = jnp.concatenate([turned, mask, jnp.full((ROWS, HEADS, 1), -MASKED, bf16), jnp.zeros((ROWS, HEADS, 23), bf16)], axis=2)
     even = jnp.concatenate([plain[:, 0::2], extra[:, 0::2]], axis=2)
     odd = jnp.concatenate([extra[:, 1::2], plain[:, 1::2]], axis=2)
     query = jnp.stack([even, odd], axis=2).reshape(ROWS, HEADS, 128).transpose(1, 2, 0)
@@ -519,8 +628,13 @@
         scratch_shapes=[
             pltpu.VMEM((2, PLANE, 2, PIECE, LATENT), bf16),
             pltpu.VMEM((HEADS, 1, ROWS), f32),
-            pltpu.VMEM((HEADS, 8, ROWS), f32),
-            pltpu.VMEM((HEADS, 64, ROWS), f32),
+            pltpu.VMEM((2, GROUP, STEP, ROWS), f32),
+            pltpu.VMEM((2, GROUP, 1, ROWS), f32),
+            pltpu.VMEM((HEADS, 1, ROWS), f32),
+            pltpu.VMEM((2, GROUP, STEP, ROWS), bf16),
+            pltpu.VMEM((HEADS, STEP, 128), bf16),
+            pltpu.VMEM((2, HEADS, 80, STEP), bf16),
+            pltpu.VMEM((HEADS, 80, ROWS), f32),
             pltpu.VMEM((2, HEADS * 64, HALF), bf16),
             pltpu.VMEM((2, HEADS * 64, HALF), bf16),
             pltpu.VMEM((2 * HEADS * 64, D), bf16),

time: 175 us -> 136 us (0.78)
  the two profiles are of different devices: /device:TPU:1 before, /device:TPU:12 now
where the time goes in v2:
time: 136 us; the launch traced here: 135 us
  Pallas kernels  124 us (91%)
  local copies, waits for them, and re-layouts  7.33 us (5%)
  other arithmetic  4.2 us (3%)
    pallas_call x1, Pallas kernels, local(): pl.pallas_call(kernel, out_shape=jax.ShapeDtypeStruct((HALF, D), bf16), i...  124 us
    unnamed x10, local copies, waits for them, and re-layouts  5.52 us

profile of v2, /device:TPU:12, one launch (start us, length us, event | category | flops | bytes accessed | tf_op | source)
XLA Modules:
  0.0 135.4 jit_solution(12257452515558966297)
XLA Ops:
  0.0 0.1 pad.5.clone
  0.1 0.8 eq.29
  0.9 0.7 multiply_convert_fusion
  1.6 0.1 copy.23
  1.7 0.1 convert_convert_fusion
  1.8 0.9 fusion.5
  2.7 0.1 concatenate.30
  2.8 0.1 copy.24
  2.9 0.1 concatenate.31
  3.0 0.1 copy.25
  3.2 0.0 copy-start.1
  3.2 0.2 maximum_bitcast_fusion.2
  3.3 0.1 reshape.115
  3.4 1.4 %copy.28.route_ref = f32[128,2]{1,0:T(8,128)} copy(f32[128,2]{0,1:T(2,128)} %param.26) | data formatting | bytes 2048 | tf_op args[11]
  4.9 1.4 %copy.27.ids_ref = s32[128,2]{1,0:T(8,128)} copy(s32[128,2]{0,1:T(2,128)} %param.25) | data formatting | bytes 2048 | tf_op args[10]
  6.3 0.9 fusion.3
  7.1 0.2 concatenate.27
  7.4 0.0 copy-done.2
  7.4 0.7 pad_maximum_fusion.1.own_ref
  8.2 0.8 pad_maximum_fusion
  9.0 0.0 copy-done.1
  9.0 0.8 copy.26
  9.8 123.7 %shard_map.145 = bf16[128,2048]{1,0:T(8,128)(2,1)} custom-call(bf16[6,128,256]{2,1,0:T(8,128)(2,1)} %bitcast.21, bf16[2,160,256]{2,1,0:T(8,128)(2,1)} %pad_maximum_fusion.1.own_ref, bf16[256,384]{1,0:T(8,128)(2,1)} %key_w_ref.1, bf16[384,256]{1,0:T(8,128)(2,1)} %bitcast.22, bf16[128,2048]{1,0:T(8,128)(2,1)} %residual_ref.1, f32[1,2048]{1,0:T(1,128)} %bitcast.26, ...), custom_call_target="tpu_custom_call" | custom-call | tf_op jit(solution)/shard_map/pallas_call | solution.py:623
  133.5 1.9 %copy.30 = bf16[128,2048]{1,0:T(8,128)(2,1)} copy(bf16[128,2048]{1,0:T(8,128)(2,1)} %shard_map.145) | data formatting | bytes 1048576
  (13 shorter events, 0.1 us)
Async XLA Ops:
  0.0 7.4 %copy-start.2 = (bf16[256,256]{1,0:T(8,128)(2,1)S(1)}, bf16[256,256]{1,0:T(8,128)(2,1)}, u32[]{:S(2)}) copy-start(bf16[256,256]{1,0:T(8,128)(2,1)} %param.17) | copy-start | bytes 393220
  0.0 8.1 %copy-start = (bf16[256,576]{0,1:T(8,128)(2,1)S(1)}, bf16[256,576]{0,1:T(8,128)(2,1)}, u32[]{:S(2)}) copy-start(bf16[256,576]{0,1:T(8,128)(2,1)} %param.16) | copy-start | bytes 884740
  3.2 5.8 %copy-start.1 = (bf16[256,384]{1,0:T(8,128)(2,1)S(1)}, bf16[256,384]{1,0:T(8,128)(2,1)}, u32[]{:S(2)}) copy-start(bf16[256,384]{1,0:T(8,128)(2,1)} %param.21) | copy-start | bytes 589828

commit v3 on v2

--- a/solution.py
+++ b/solution.py
@@ -60,20 +60,12 @@
 
 ORDER = exchange_order()
 OWN_SLOT = PLANE - 1
-
-
-def rotate(source, cosine, sine_part):
-    half_width = source.shape[-1] // 2
-    upper_half = source[..., :half_width].astype(jnp.float32)
-    lower_half = source[..., half_width:].astype(jnp.float32)
-    turned = jnp.concatenate(
-        [
-            upper_half * cosine - lower_half * sine_part,
-            lower_half * cosine + upper_half * sine_part,
-        ],
-        axis=-1,
-    )
-    return turned.astype(jnp.bfloat16)
+SEQUENCE = [(0, 0), (0, 1), (1, 0), (0, 3), (3, 0), (0, 2), (2, 0), (1, 1)]
+SEQUENCE += [(1, 3), (3, 1), (3, 3), (1, 2), (2, 1), (3, 2), (2, 3), (2, 2)]
+
+
+def turned(upper, lower, cosine, sine_part):
+    return [upper * cosine - lower * sine_part, lower * cosine + upper * sine_part]
 
 
 def nn(a, b):
@@ -85,21 +77,27 @@
 
 
 def kernel(
-    query_ref,
-    own_ref,
+    raw_query_ref,
+    latent_ref,
+    rope_ref,
+    doc_ref,
+    cosine_ref,
+    sine_ref,
     key_w_ref,
-    value_w_ref,
+    raw_value_w_ref,
     residual_ref,
     mix_gain_ref,
     moe_gain_ref,
     ids_ref,
-    ids_t_ref,
     route_ref,
     proj_hbm,
     gate_hbm,
     up_hbm,
     down_hbm,
     out_ref,
+    own_ref,
+    query_ref,
+    value_w_ref,
     kv,
     run_max,
     held,
@@ -123,7 +121,8 @@
     done_buf,
     back_buf,
     z_send,
-    plane_send,
+    first_send,
+    second_send,
     pass_send,
     got,
     passed,
@@ -143,6 +142,7 @@
     other = 1 - tp
     z = sp // PLANE
     me = sp % PLANE
+    y, x = me // DEPTH, me % DEPTH
 
     def remote(src, dst, send_sem, recv_sem, device):
         return pltpu.make_async_remote_copy(
@@ -174,6 +174,22 @@
     for copy in local_copies:
         copy.start()
 
+    cosine, sine_part = cosine_ref[...], sine_ref[...]
+    rope = rope_ref[...].astype(jnp.float32)
+    hot = (lax.broadcasted_iota(jnp.int32, (8, ROWS), 0) == doc_ref[...]).astype(jnp.float32)
+    extra = turned(rope[:16, :], rope[16:, :], cosine, sine_part) + [hot, jnp.zeros((24, ROWS), jnp.float32)]
+    extra = jnp.concatenate(extra + extra, axis=0).T.astype(jnp.bfloat16)
+    low_quarter = lax.broadcasted_iota(jnp.int32, (PIECE - HALF, 128), 1) < 64
+    for half in range(2):
+        own_ref[half, :HALF, :] = latent_ref[HALF * half : HALF * half + HALF, :]
+        for tile in range(2):
+            at = HALF * half + 64 * tile
+            own_ref[half, HALF:PIECE, 128 * tile : 128 * tile + 128] = jnp.where(
+                low_quarter, extra[at : at + 32, :], extra[at + 32 : at + 64, :]
+            )
+    keep = pltpu.make_async_copy(own_ref.at[tp], kv.at[2, me, tp], own_copy)
+    keep.start()
+    keep.wait()
     pl.semaphore_wait(barrier, EXPERTS)
 
     next_z = []
@@ -189,24 +205,44 @@
         copy.start()
         next_z.append(copy)
 
-    def plane_copy(kind, step, own):
-        peer = (me + step) % PLANE
+    def place(dy, dx):
+        return ((y + dy + DEPTH) % DEPTH) * DEPTH + (x + dx + DEPTH) % DEPTH
+
+    def first_peer(k):
+        return jnp.where(tp == 0, place(k, 0), place(0, k))
+
+    def second_peer(k):
+        return jnp.where(tp == 0, place(0, k), place(k, 0))
+
+    def first_copy(kind, k):
+        peer = first_peer(k)
+        later = peer > me
+        source = (0, jnp.where(later, 2, 1), jnp.where(later, 1, 2))[kind]
         return remote(
-            own_ref.at[tp] if own else kv.at[kind, me, tp],
+            kv.at[source, me, tp],
             kv.at[kind, me, tp],
-            plane_send.at[kind, step],
+            first_send.at[kind, k],
             got.at[kind, me],
             (z * PLANE + peer, tp),
         )
 
-    def send_own(step, carry):
-        @pl.when((me + step) % PLANE > me)
-        def _():
-            plane_copy(1, step, True).start()
-
-        return carry
-
-    lax.fori_loop(1, PLANE, send_own, 0)
+    def second_copy(kind, k, j):
+        peer = second_peer(k)
+        later = peer > me
+        origin = first_peer(-j)
+        if kind == 0:
+            source = 0
+        elif j == 0:
+            source = jnp.where(later, 2, 1)
+        else:
+            source = jnp.where((tp == 1) & ((origin < me) != later), 2, 1)
+        return remote(
+            kv.at[source, origin, tp],
+            kv.at[kind, origin, tp],
+            second_send.at[kind, k, j],
+            got.at[kind, origin],
+            (z * PLANE + peer, tp),
+        )
 
     weight_copies = [
         remote(src.at[0], dst.at[tp], weight_send.at[i], weight_got.at[i], (sp, other))
@@ -215,6 +251,18 @@
     for copy in weight_copies:
         copy.start()
 
+    mask = (hot - 1.0) * MASKED
+    dead_row = jnp.where(lax.broadcasted_iota(jnp.int32, (24, ROWS), 0) == 0, -MASKED, 0.0)
+    flat = raw_query_ref[...].astype(jnp.float32)
+    for head in range(HEADS):
+        at = (UNROTATED_DIM + ROPE) * head
+        plain = [flat[at : at + 64, :]]
+        rest = turned(flat[at + 64 : at + 80, :], flat[at + 80 : at + 96, :], cosine, sine_part)
+        rest = rest + [mask, dead_row]
+        query_ref[head] = jnp.concatenate(
+            plain + rest if head % 2 == 0 else rest + plain, axis=0
+        ).astype(jnp.bfloat16)
+    value_w_ref[...] = raw_value_w_ref[...].astype(jnp.float32).T.astype(jnp.bfloat16)
     values[...] = jnp.ones_like(values)
     low_lanes = lax.broadcasted_iota(jnp.int32, (HALF, 128), 1) < 64
     dead_lane = (lax.broadcasted_iota(jnp.int32, (PIECE - HALF, 128), 1) % 64 == DEAD).astype(
@@ -309,44 +357,63 @@
             kv.at[kind, source, tp], kv.at[kind, source, tp], got.at[kind, source]
         )
 
-    arrival(0, me).wait()
-    pass_copy(0, me).start()
-
-    def send_first(step, carry):
-        plane_copy(0, step, False).start()
-        return carry
-
-    lax.fori_loop(1, PLANE, send_first, 0)
-    arrival(1, me).wait()
-    pass_copy(1, me).start()
-
-    def send_second(step, carry):
-        @pl.when((me + step) % PLANE < me)
+    def take(origin):
+        for kind in range(2):
+            arrival(kind, origin).wait()
+            pass_copy(kind, origin).start()
+
+    def relay(j):
+        origin = first_peer(-j)
+        take(origin)
+
+        @pl.when(tp == 1)
         def _():
-            plane_copy(1, step, False).start()
-
-        return carry
-
-    lax.fori_loop(1, PLANE, send_second, 0)
-    before = (me - 1 + PLANE) % PLANE
-    for kind in range(2):
-        arrival(kind, before).wait()
-        pass_copy(kind, before).start()
-
-    steps = jnp.where(z >= 1, PLANE // 2, me // 2 + 1)
+            arrival(2, origin).wait()
+
+        for k in (1, 3, 2):
+            for kind in range(2):
+                second_copy(kind, k, j).start()
+
+    take(me)
+    for k in (1, 3, 2):
+        for kind in range(2):
+            first_copy(kind, k).start()
+
+        @pl.when(tp == 1)
+        def _():
+            first_copy(2, k).start()
+
+        for kind in range(2):
+            second_copy(kind, k, 0).start()
+    for j in (1, 3):
+        relay(j)
+        take(second_peer(-j))
+
     last_slot = (GROUPS - 1) % 2
     last_head = (GROUPS - 1) * GROUP
 
     def visit(step, carry):
-        sources = [(me - 2 * step - i + PLANE) % PLANE for i in range(2)]
-
-        @pl.when(step < PLANE // 2 - 1)
+        @pl.when(step == 0)
         def _():
-            for i in range(2):
-                later = (me - 2 * step - 2 - i + PLANE) % PLANE
-                for kind in range(2):
-                    arrival(kind, later).wait()
-                    pass_copy(kind, later).start()
+            relay(2)
+            take(second_peer(-2))
+
+        for n in range(1, len(SEQUENCE) // 2 - 1):
+            ahead = [o for o in SEQUENCE[2 * n + 2 : 2 * n + 4] if o[0] and o[1]]
+            if ahead:
+
+                @pl.when(step == n)
+                def _(ahead=ahead):
+                    for dy, dx in ahead:
+                        take(place(-dy, -dx))
+
+        sources = []
+        for i in range(2):
+            dy, dx = 0, 0
+            for n in range(len(SEQUENCE) // 2):
+                dy = jnp.where(step == n, SEQUENCE[2 * n + i][0], dy)
+                dx = jnp.where(step == n, SEQUENCE[2 * n + i][1], dx)
+            sources.append(place(-dy, -dx))
 
         for source in sources:
             for kind in range(2):
@@ -354,7 +421,7 @@
                     kv.at[kind, source, other], kv.at[kind, source, other], passed.at[kind, source]
                 ).wait()
 
-        @pl.when(step < steps)
+        @pl.when(step >= 0)
         def _():
             bank = step % 2
             blocks, dead = [], []
@@ -425,7 +492,8 @@
     at_row = lax.broadcasted_iota(jnp.int32, (HALF, HALF), 0)
     at_col = lax.broadcasted_iota(jnp.int32, (HALF, HALF), 1)
     expert_row = lax.broadcasted_iota(jnp.int32, (EXPERTS, HALF), 0)
-    hot = [(expert_row == ids_t_ref[k : k + 1, :]).astype(jnp.float32) for k in range(2)]
+    ids_t = ids_ref[...]
+    hot = [(expert_row == ids_t[k : k + 1, :]).astype(jnp.float32) for k in range(2)]
     earlier = nn(
         (hot[0] + hot[1]).astype(jnp.bfloat16), (at_row < at_col).astype(jnp.float32).astype(jnp.bfloat16)
     )
@@ -433,15 +501,13 @@
     chooser = jnp.zeros((EXPERTS * CAP, HALF), jnp.float32)
     for k in range(2):
         rank = jnp.sum(hot[k] * earlier, axis=0, keepdims=True).astype(jnp.int32)
-        slot = ids_t_ref[k : k + 1, :] * CAP + rank
+        slot = ids_t[k : k + 1, :] * CAP + rank
         chooser = chooser + (slot_row == slot).astype(jnp.float32)
     chooser = chooser.astype(jnp.bfloat16)
     for n in range(8):
         cols = slice(256 * n, 256 * n + 256)
         picked = nn(chooser, normed[:, cols]).astype(jnp.bfloat16)
         send_buf[:, :, cols] = picked.reshape(EXPERTS, CAP, 256)
-
-    y, x = me // DEPTH, me % DEPTH
 
     def toward(offset, sign):
         dz, dy, dx = offset
@@ -522,7 +588,10 @@
     mine_back.start()
 
     expert_col = lax.broadcasted_iota(jnp.int32, (HALF, EXPERTS), 1)
-    hot = [(expert_col == ids_ref[:, k : k + 1]).astype(jnp.float32) for k in range(2)]
+    routes = [ids_t.astype(jnp.float32), route_ref[...], jnp.zeros((HALF - 4, HALF), jnp.float32)]
+    routes = jnp.concatenate(routes, axis=0).T
+    ids = routes[:, :2].astype(jnp.int32)
+    hot = [(expert_col == ids[:, k : k + 1]).astype(jnp.float32) for k in range(2)]
     earlier = nn(
         (at_col < at_row).astype(jnp.float32).astype(jnp.bfloat16), (hot[0] + hot[1]).astype(jnp.bfloat16)
     )
@@ -530,7 +599,7 @@
     takers = []
     for k in range(2):
         rank = jnp.sum(hot[k] * earlier, axis=1, keepdims=True).astype(jnp.int32)
-        slot = ids_ref[:, k : k + 1] * CAP + rank
+        slot = ids[:, k : k + 1] * CAP + rank
         takers.append((slot_col == slot).astype(jnp.float32).astype(jnp.bfloat16))
 
     mine_back.wait()
@@ -547,7 +616,7 @@
         cols = slice(512 * n, 512 * n + 512)
         came = back_buf[:, :, cols].reshape(EXPERTS * CAP, 512)
         both = (
-            nn(takers[0], came) * route_ref[:, 0:1] + nn(takers[1], came) * route_ref[:, 1:2]
+            nn(takers[0], came) * routes[:, 2:3] + nn(takers[1], came) * routes[:, 3:4]
         )
         out_ref[:, cols] = (middle[:, cols].astype(jnp.float32) + both).astype(jnp.bfloat16)
 
@@ -557,12 +626,15 @@
         copy.wait_send()
     heads_copy.wait_send()
 
-    def plane_done(step, carry):
-        plane_copy(0, step, True).wait_send()
-        plane_copy(1, step, True).wait_send()
-        return carry
-
-    lax.fori_loop(1, PLANE, plane_done, 0)
+    for k in (1, 2, 3):
+        for kind in range(2):
+            first_copy(kind, k).wait_send()
+            for j in range(DEPTH):
+                second_copy(kind, k, j).wait_send()
+
+        @pl.when(tp == 1)
+        def _():
+            first_copy(2, k).wait_send()
 
     def pass_done(source, carry):
         pass_copy(0, source).wait_send()
@@ -598,24 +670,7 @@
     positions = (first + jnp.arange(ROWS, dtype=jnp.int32)).astype(f32)
     half_width = ROPE // 2
     frequency = rope_base ** (-jnp.arange(half_width, dtype=f32) / half_width)
-    angles = positions[:, None] * frequency[None, :]
-    cosine, sine_part = jnp.cos(angles), jnp.sin(angles)
-    hot = (doc_ids[:, None] == jnp.arange(8, dtype=jnp.int32)[None, :]).astype(f32)
-    key_extra = jnp.concatenate(
-        [rotate(rope_key, cosine, sine_part), hot.astype(bf16), jnp.zeros((ROWS, 24), bf16)], axis=1
-    )
-    key_extra = (
-        key_extra.reshape(2, 4, 32, 64).transpose(0, 2, 1, 3).reshape(2, PIECE - HALF, LATENT)
-    )
-    own = jnp.concatenate([latent.reshape(2, HALF, LATENT), key_extra], axis=1)
-    shaped = queries.reshape(ROWS, HEADS, UNROTATED_DIM + ROPE)
-    plain = shaped[..., :UNROTATED_DIM]
-    turned = rotate(shaped[..., UNROTATED_DIM:], cosine[:, None, :], sine_part[:, None, :])
-    mask = jnp.broadcast_to(((hot - 1.0) * MASKED).astype(bf16)[:, None, :], (ROWS, HEADS, 8))
-    extra = jnp.concatenate([turned, mask, jnp.full((ROWS, HEADS, 1), -MASKED, bf16), jnp.zeros((ROWS, HEADS, 23), bf16)], axis=2)
-    even = jnp.concatenate([plain[:, 0::2], extra[:, 0::2]], axis=2)
-    odd = jnp.concatenate([extra[:, 1::2], plain[:, 1::2]], axis=2)
-    query = jnp.stack([even, odd], axis=2).reshape(ROWS, HEADS, 128).transpose(1, 2, 0)
+    angles = positions[None, :] * frequency[:, None]
 
     vmem = pl.BlockSpec(memory_space=pltpu.VMEM)
     anywhere = pl.BlockSpec(memory_space=pl.ANY)
@@ -623,10 +678,13 @@
     return pl.pallas_call(
         kernel,
         out_shape=jax.ShapeDtypeStruct((HALF, D), bf16),
-        in_specs=[vmem] * 10 + [anywhere] * 4,
+        in_specs=[vmem] * 13 + [anywhere] * 4,
         out_specs=vmem,
         scratch_shapes=[
-            pltpu.VMEM((2, PLANE, 2, PIECE, LATENT), bf16),
+            pltpu.VMEM((2, PIECE, LATENT), bf16),
+            pltpu.VMEM((HEADS, 128, ROWS), bf16),
+            pltpu.VMEM((HEADS * 64, LATENT), bf16),
+            pltpu.VMEM((3, PLANE, 2, PIECE, LATENT), bf16),
             pltpu.VMEM((HEADS, 1, ROWS), f32),
             pltpu.VMEM((2, GROUP, STEP, ROWS), f32),
             pltpu.VMEM((2, GROUP, 1, ROWS), f32),
@@ -649,9 +707,10 @@
             pltpu.VMEM((EXPERTS, CAP, D), bf16),
             pltpu.VMEM((EXPERTS, CAP, D), bf16),
             dma((2,)),
+            dma((3, DEPTH)),
+            dma((2, DEPTH, DEPTH)),
             dma((2, PLANE)),
-            dma((2, PLANE)),
-            dma((2, PLANE)),
+            dma((3, PLANE)),
             dma((2, PLANE)),
             dma((4,)),
             dma((3,)),
@@ -668,16 +727,19 @@
             collective_id=0, has_side_effects=True, vmem_limit_bytes=60 * 1024 * 1024
         ),
     )(
-        query,
-        own,
+        queries.T,
+        latent,
+        rope_key.T,
+        doc_ids.reshape(1, ROWS),
+        jnp.cos(angles),
+        jnp.sin(angles),
         latent_to_key,
-        latent_to_value.T,
+        latent_to_value,
         residual,
         mix_gain.reshape(1, D),
         moe_gain.reshape(1, D),
-        expert_ids,
         expert_ids.T,
-        route_weight,
+        route_weight.T,
         out_proj,
         gate_weight,
         up_weight,

time: 136 us -> 114 us (0.84)
  the two profiles are of different devices: /device:TPU:12 before, /device:TPU:1 now
where the time goes in v3:
time: 114 us; the launch traced here: 113 us
  Pallas kernels  111 us (97%)
  local copies, waits for them, and re-layouts  1.88 us (2%)
    pallas_call x1, Pallas kernels, local(): pl.pallas_call(kernel, out_shape=jax.ShapeDtypeStruct((HALF, D), bf16), i...  111 us

profile of v3, /device:TPU:1, one launch (start us, length us, event | category | flops | bytes accessed | tf_op | source)
XLA Modules:
  0.0 113.4 jit_solution(10951844042175674673)
XLA Ops:
  0.0 0.8 multiply_sine_fusion
  0.8 110.7 %shard_map.145 = bf16[128,2048]{1,0:T(8,128)(2,1)} custom-call(bf16[576,256]{1,0:T(8,128)(2,1)} %bitcast.7, bf16[256,256]{1,0:T(8,128)(2,1)} %latent_ref.1, bf16[32,256]{1,0:T(8,128)(2,1)} %bitcast.8, s32[1,256]{1,0:T(1,128)} %bitcast.11, f32[16,256]{1,0:T(8,128)} %get-tuple-element.6.cosine_ref, f32[16,256]{1,0:T(8,128)} %get-tuple-element.5.sine_ref, ...), custom_call_target="tpu_custom_call" | custom-call | tf_op jit(solution)/shard_map/pallas_call | solution.py:678
  111.5 1.9 %copy.17 = bf16[128,2048]{1,0:T(8,128)(2,1)} copy(bf16[128,2048]{1,0:T(8,128)(2,1)} %shard_map.145) | data formatting | bytes 1048576
  (2 shorter events, 0.0 us)

commit v4 on v3

--- a/solution.py
+++ b/solution.py
@@ -375,16 +375,24 @@
                 second_copy(kind, k, j).start()
 
     take(me)
-    for k in (1, 3, 2):
+    for k in (1, 3):
         for kind in range(2):
             first_copy(kind, k).start()
-
-        @pl.when(tp == 1)
-        def _():
+            second_copy(kind, k, 0).start()
+
+    @pl.when(tp == 1)
+    def _():
+        for k in (1, 3):
             first_copy(2, k).start()
 
-        for kind in range(2):
-            second_copy(kind, k, 0).start()
+    for kind in range(2):
+        first_copy(kind, 2).start()
+        second_copy(kind, 2, 0).start()
+
+    @pl.when(tp == 1)
+    def _():
+        first_copy(2, 2).start()
+
     for j in (1, 3):
         relay(j)
         take(second_peer(-j))
@@ -392,7 +400,7 @@
     last_slot = (GROUPS - 1) % 2
     last_head = (GROUPS - 1) * GROUP
 
-    def visit(step, carry):
+    def errands(step):
         @pl.when(step == 0)
         def _():
             relay(2)
@@ -407,6 +415,7 @@
                     for dy, dx in ahead:
                         take(place(-dy, -dx))
 
+    def visit(step, carry):
         sources = []
         for i in range(2):
             dy, dx = 0, 0
@@ -436,6 +445,8 @@
             score(0, 0, STEP, False)
 
             for j in range(GROUPS - 1):
+                if j == 1:
+                    errands(step)
 
                 @pl.when(step >= -1 - j)
                 def _(j=j):
@@ -677,7 +688,7 @@
     dma = pltpu.SemaphoreType.DMA
     return pl.pallas_call(
         kernel,
-        out_shape=jax.ShapeDtypeStruct((HALF, D), bf16),
+        out_shape=pltpu.VMEM((HALF, D), bf16),
         in_specs=[vmem] * 13 + [anywhere] * 4,
         out_specs=vmem,
         scratch_shapes=[

time: 114 us -> 108 us (0.947)
  Pallas kernels: 111 us -> 106 us
    pallas_call x1, Pallas kernels: 111 us -> 106 us  [local(): pl.pallas_call(kernel, out_shape=pltpu.VMEM((HALF, D), bf16), in_specs=[v...]
where the time goes in v4:
time: 108 us
  Pallas kernels  106 us (98%)
    pallas_call x1, Pallas kernels, local(): pl.pallas_call(kernel, out_shape=pltpu.VMEM((HALF, D), bf16), in_specs=[v...  106 us

profile of v4, /device:TPU:1, one launch (start us, length us, event | category | flops | bytes accessed | tf_op | source)
XLA Modules:
  0.0 107.5 jit_solution(18344027362850428849)
XLA Ops:
  0.0 0.8 multiply_sine_fusion
  0.8 105.9 %shard_map.145 = bf16[128,2048]{1,0:T(8,128)(2,1)S(1)} custom-call(bf16[576,256]{1,0:T(8,128)(2,1)} %bitcast.7, bf16[256,256]{1,0:T(8,128)(2,1)} %latent_ref.1, bf16[32,256]{1,0:T(8,128)(2,1)} %bitcast.8, s32[1,256]{1,0:T(1,128)} %bitcast.11, f32[16,256]{1,0:T(8,128)} %get-tuple-element.6.cosine_ref, f32[16,256]{1,0:T(8,128)} %get-tuple-element.5.sine_ref, ...), custom_call_target="tpu_custom_call" | custom-call | tf_op jit(solution)/shard_map/pallas_call | solution.py:689
  106.7 0.8 copy.17
  (2 shorter events, 0.0 us)

commit v5 on v4

--- a/solution.py
+++ b/solution.py
@@ -22,7 +22,7 @@
 DEPTH = 4
 GROUP = 2
 GROUPS = HEADS // GROUP
-CHUNK = 64
+CHUNK = 128
 STEP = 4 * ROWS
 DEAD = 40
 rope_base = 10000.0
@@ -136,6 +136,8 @@
     own_copy,
     back_send,
     back_got,
+    plane_in,
+    all_in,
 ):
     sp = lax.axis_index("sp")
     tp = lax.axis_index("tp")
@@ -154,16 +156,16 @@
             device_id_type=MESH,
         )
 
+    def in_line(axis, k):
+        at = [z, y, x]
+        at[axis] = (at[axis] + k) % DEPTH
+        return (at[0] * PLANE + at[1] * DEPTH + at[2], tp)
+
     barrier = pltpu.get_barrier_semaphore()
     pl.semaphore_signal(barrier, inc=1, device_id=(sp, other), device_id_type=MESH)
-
-    def greet(step, carry):
-        pl.semaphore_signal(
-            barrier, inc=1, device_id=((sp + step) % EXPERTS, tp), device_id_type=MESH
-        )
-        return carry
-
-    lax.fori_loop(1, EXPERTS, greet, 0)
+    for axis in range(3):
+        for k in range(1, DEPTH):
+            pl.semaphore_signal(barrier, inc=1, device_id=in_line(axis, k), device_id_type=MESH)
 
     local_copies = [
         pltpu.make_async_copy(proj_hbm, proj, weight_local.at[0]),
@@ -190,7 +192,9 @@
     keep = pltpu.make_async_copy(own_ref.at[tp], kv.at[2, me, tp], own_copy)
     keep.start()
     keep.wait()
-    pl.semaphore_wait(barrier, EXPERTS)
+    pl.semaphore_wait(barrier, 3 * (DEPTH - 1) + 1)
+    for k in range(1, DEPTH):
+        pl.semaphore_signal(plane_in, inc=1, device_id=in_line(2, k), device_id_type=MESH)
 
     next_z = []
     for hop in (1, 2):
@@ -397,6 +401,10 @@
         relay(j)
         take(second_peer(-j))
 
+    pl.semaphore_wait(plane_in, DEPTH - 1)
+    for k in range(1, DEPTH):
+        pl.semaphore_signal(all_in, inc=1, device_id=in_line(0, k), device_id_type=MESH)
+
     last_slot = (GROUPS - 1) % 2
     last_head = (GROUPS - 1) * GROUP
 
@@ -542,6 +550,7 @@
             done_buf.at[slot], back_buf.at[sp], back_send.at[slot], back_got.at[sp], (source, tp)
         )
 
+    pl.semaphore_wait(all_in, DEPTH - 1)
     away = [(kind, i) for kind in range(DEPTH) for i in range(PLANE) if any(ORDER[kind][i])]
     for kind, i in away:
         go_copy(kind, i).start()
@@ -733,6 +742,8 @@
             dma,
             dma((EXPERTS,)),
             dma((EXPERTS,)),
+            pltpu.SemaphoreType.REGULAR,
+            pltpu.SemaphoreType.REGULAR,
         ],
         compiler_params=pltpu.CompilerParams(
             collective_id=0, has_side_effects=True, vmem_limit_bytes=60 * 1024 * 1024

time: 108 us -> 106 us (0.981)
  Pallas kernels: 106 us -> 104 us
    pallas_call x1, Pallas kernels: 106 us -> 104 us  [local(): pl.pallas_call(kernel, out_shape=pltpu.VMEM((HALF, D), bf16), in_specs=[v...]
where the time goes in v5:
time: 106 us
  Pallas kernels  104 us (98%)
    pallas_call x1, Pallas kernels, local(): pl.pallas_call(kernel, out_shape=pltpu.VMEM((HALF, D), bf16), in_specs=[v...  104 us

profile of v5, /device:TPU:1, one launch (start us, length us, event | category | flops | bytes accessed | tf_op | source)
XLA Modules:
  0.0 106.0 jit_solution(3924986313762349892)
XLA Ops:
  0.0 0.8 multiply_sine_fusion
  0.8 104.4 %shard_map.145 = bf16[128,2048]{1,0:T(8,128)(2,1)S(1)} custom-call(bf16[576,256]{1,0:T(8,128)(2,1)} %bitcast.7, bf16[256,256]{1,0:T(8,128)(2,1)} %latent_ref.1, bf16[32,256]{1,0:T(8,128)(2,1)} %bitcast.8, s32[1,256]{1,0:T(1,128)} %bitcast.11, f32[16,256]{1,0:T(8,128)} %get-tuple-element.6.cosine_ref, f32[16,256]{1,0:T(8,128)} %get-tuple-element.5.sine_ref, ...), custom_call_target="tpu_custom_call" | custom-call | tf_op jit(solution)/shard_map/pallas_call | solution.py:698
  105.2 0.8 copy.17
  (2 shorter events, 0.0 us)
